TPU v7x, 32 devices: a whole 2x2x4 slice. The times are simulated.
32 devices in a mesh: sp: 16 (over z, y, x), tp: 2 (over core).
Axes of the slice: x: 2, y: 2, z: 4, core: 2. Of those that a mesh axis runs over, the one named last changes fastest.
Arguments:
- resid: bfloat16 [4096, 2048], P(('sp', 'tp')), may hold values from -3 to 3
- queries: bfloat16 [4096, 1024], P('sp', 'tp'), may hold values from -8 to 8
- keys: bfloat16 [4096, 256], P('sp', 'tp'), may hold values from -8 to 8
- values: bfloat16 [4096, 256], P('sp', 'tp'), may hold values from -6 to 6
- docs: int32 [4096], P('sp'), may hold values from 0 to 3, never falling along the last dimension, each value on 1 to 2048 neighbouring positions
- sink: float32 [8], P('tp'), may hold values from 2 to 6
- w_out: bfloat16 [1024, 2048], replicated, may hold values from -0.375 to 0.375
- norm_gain: float32 [2048], replicated, may hold values from 0.1 to 1.9
- w_gate: bfloat16 [16, 2048, 1024], P('sp', None, 'tp'), may hold values from -0.125 to 0.125
- w_up: bfloat16 [16, 2048, 1024], P('sp', None, 'tp'), may hold values from -0.125 to 0.125
- w_down: bfloat16 [16, 1024, 2048], P('sp', 'tp'), may hold values from -0.1875 to 0.1875
- expert_ids: int32 [4096, 2], P(('sp', 'tp')), may hold values from 0 to 15, all different within a row; in each aligned block of 128 rows (0 to 127, 128 to 255, ...) at most 32 rows name the same one
- route_weights: float32 [4096, 2], P(('sp', 'tp')), may hold values from 0.1 to 0.9
Outputs:
- layer_out: bfloat16 [4096, 2048], P(('sp', 'tp'))
Inputs may be any that keep to these rules, and one draw needn't show every extreme that they name: `docs`: document numbers never fall along the sequence; a document holds at most 2048 positions. `expert_ids`: each row names 2 different experts. The rows of one device (aligned blocks of 256 // 2 rows) name one expert at most 32 times, and in every draw some expert is named exactly 32 times by some device.
All inputs are finite; a program needn't handle non-finite values.
Results may differ from a plain program's by a relative error of at most 0.007.
Values may be sent and summed in bfloat16 or wider, within the bound.
A program may use at most 128 MiB of HBM per device.

v0:
```python
import jax
import jax.numpy as jnp
from jax import lax
from jax.sharding import PartitionSpec as P

HEAD_WIDTH = 128
WINDOW_RADIUS = 128


eps = 1e-06


def with_halo(cells, sides, width):
    for axis, dim in sides:
        count = lax.axis_size(axis)
        ends = count - 1
        head = lax.slice_in_dim(cells, 0, width, axis=dim)
        tail = lax.slice_in_dim(cells, cells.shape[dim] - width, cells.shape[dim], axis=dim)
        cells = jnp.concatenate(
            [
                lax.ppermute(tail, axis, [(i, (i + 1) % count) for i in range(ends)]),
                cells,
                lax.ppermute(head, axis, [((i + 1) % count, i) for i in range(ends)]),
            ],
            axis=dim,
        )
    return cells


def window_band(table):
    return jnp.concatenate([table[:-2], table[1:-1], table[2:]], axis=1)


def local(
    resid,
    queries,
    keys,
    values,
    docs,
    sink,
    w_out,
    norm_gain,
    w_gate,
    w_up,
    w_down,
    expert_ids,
    route_weights,
):
    rows_all = queries.shape[0]
    kv_local = keys.shape[1] // HEAD_WIDTH
    q_local = queries.shape[1] // HEAD_WIDTH
    head_group = q_local // kv_local
    n_sp = lax.axis_size("sp")
    n_tp = lax.axis_size("tp")
    total = n_sp * rows_all
    offset = lax.axis_index("sp") * rows_all
    query_blocks = rows_all // WINDOW_RADIUS
    whole_gate, whole_up, whole_down = (
        lax.all_gather(w_gate, "tp", axis=2, tiled=True),
        lax.all_gather(w_up, "tp", axis=2, tiled=True),
        lax.all_gather(w_down, "tp", axis=1, tiled=True),
    )
    doc_marks = docs.astype(jnp.bfloat16)
    padk, padv, padd = (
        with_halo(keys, (("sp", 0),), WINDOW_RADIUS),
        with_halo(values, (("sp", 0),), WINDOW_RADIUS),
        with_halo(doc_marks, (("sp", 0),), WINDOW_RADIUS),
    )
    key_band = window_band(padk.reshape(query_blocks + 2, WINDOW_RADIUS, kv_local, HEAD_WIDTH))
    value_band = window_band(padv.reshape(query_blocks + 2, WINDOW_RADIUS, kv_local, HEAD_WIDTH))
    doc_band = window_band(padd.reshape(query_blocks + 2, WINDOW_RADIUS))
    qpos = jnp.arange(query_blocks)[:, None] * WINDOW_RADIUS + jnp.arange(WINDOW_RADIUS)[None, :]
    kpos = (jnp.arange(query_blocks)[:, None] - 1) * WINDOW_RADIUS + jnp.arange(3 * WINDOW_RADIUS)[
        None, :
    ]
    where_key = offset + kpos
    inside = (where_key >= 0) & (where_key < total)
    distance = kpos[:, None, :] - qpos[:, :, None]
    qdoc = doc_marks.reshape(query_blocks, WINDOW_RADIUS)
    valid = (
        (jnp.abs(distance) <= WINDOW_RADIUS)
        & inside[:, None, :]
        & (doc_band[:, None, :] == qdoc[:, :, None])
    )
    valid = valid[:, None, None]
    query_block = queries.reshape(query_blocks, WINDOW_RADIUS, kv_local, head_group, HEAD_WIDTH)
    scores = jnp.einsum(
        "nqhgd,nkhd->nhgqk", query_block, key_band, preferred_element_type=jnp.float32
    ) * HEAD_WIDTH ** (-0.5)
    sink_logits = sink.reshape(1, kv_local, head_group, 1, 1)
    top = jnp.maximum(
        jnp.max(jnp.where(valid, scores, -jnp.inf), axis=-1, keepdims=True), sink_logits
    )
    expo = jnp.where(valid, jnp.exp(scores - top), 0.0)
    denom = jnp.sum(expo, axis=-1, keepdims=True) + jnp.exp(sink_logits - top)
    probs = (expo / denom).astype(jnp.bfloat16)
    attended = jnp.einsum(
        "nhgqk,nkhd->nqhgd", probs, value_band, preferred_element_type=jnp.float32
    ).astype(jnp.bfloat16)
    attended = attended.reshape(rows_all, q_local * HEAD_WIDTH)
    width = attended.shape[1]
    keep = rows_all // n_tp
    w_rows = lax.dynamic_slice_in_dim(w_out, lax.axis_index("tp") * width, width, 0)
    projected = lax.psum_scatter(
        jnp.dot(attended, w_rows, preferred_element_type=jnp.float32),
        "tp",
        scatter_dimension=0,
        tiled=True,
    )
    mixed = resid.astype(jnp.float32) + projected
    width_d = mixed.shape[1]
    normed = (
        mixed * lax.rsqrt(jnp.mean(mixed * mixed, axis=-1, keepdims=True) + eps) * norm_gain
    ).astype(jnp.bfloat16)
    top_k = expert_ids.shape[1]
    cap = rows_all * top_k // n_sp
    flat = expert_ids.reshape(-1)
    onehot = (flat[:, None] == jnp.arange(n_sp, dtype=jnp.int32)[None, :]).astype(jnp.int32)
    rank = jnp.sum((jnp.cumsum(onehot, axis=0) - onehot) * onehot, axis=1)
    slot = flat * cap + rank
    owner = jnp.arange(flat.shape[0], dtype=jnp.int32) // top_k
    outgoing = jnp.zeros((n_sp * cap, width_d), jnp.bfloat16).at[slot].set(normed[owner])
    landed = lax.all_to_all(outgoing, "sp", split_axis=0, concat_axis=0, tiled=True)
    hidden = (
        jax.nn.silu(jnp.dot(landed, whole_gate[0], preferred_element_type=jnp.float32))
        * jnp.dot(landed, whole_up[0], preferred_element_type=jnp.float32)
    ).astype(jnp.bfloat16)
    part = hidden.shape[1] // n_tp
    summed = jnp.zeros((landed.shape[0], width_d), jnp.float32)
    for piece in range(n_tp):
        partial_value = jnp.dot(
            hidden[:, piece * part : (piece + 1) * part],
            whole_down[0][piece * part : (piece + 1) * part],
            preferred_element_type=jnp.float32,
        ).astype(jnp.bfloat16)
        summed = summed + partial_value.astype(jnp.float32)
    returning = summed.astype(jnp.bfloat16)
    back = lax.all_to_all(returning, "sp", split_axis=0, concat_axis=0, tiled=True)
    got = back[slot].astype(jnp.float32).reshape(keep, top_k, width_d)
    extra = jnp.sum(route_weights[:, :, None] * got, axis=1)
    return (mixed + extra).astype(jnp.bfloat16)


def solution(mesh):
    in_specs = (
        P(("sp", "tp"), None),
        P("sp", "tp"),
        P("sp", "tp"),
        P("sp", "tp"),
        P("sp"),
        P("tp"),
        P(),
        P(),
        P("sp", None, "tp"),
        P("sp", None, "tp"),
        P("sp", "tp", None),
        P(("sp", "tp"), None),
        P(("sp", "tp"), None),
    )
    out_specs = P(("sp", "tp"), None)
    return jax.shard_map(local, mesh=mesh, in_specs=in_specs, out_specs=out_specs, check_vma=False)
```

profile of v0, /device:TPU:12, one launch (start us, length us, event | category | flops | bytes accessed | tf_op | source)
XLA Modules:
  0.0 203.6 jit_solution(8400333342944806731)
XLA Ops:
  6.5 0.7 convert_element_type.57
  7.2 3.4 %collective-permute-start.2 = (bf16[128]{0:T(256)(128)(2,1)S(1)}, bf16[128]{0:T(256)(128)(2,1)S(1)}, u32[]{:S(2)}, u32[]{:S(2)}) collective-permute-start(bf16[128]{0:T(256)(128)(2,1)S(1)} %get-tuple-element.15), channel_id=1, source_target_pairs={{0,2},{2,4},{4,6},{6,8},{8,10},{10,12},{12,14},{14,16},{16,18},{18... | collective-permute-start | bytes 776 | tf_op jit(solution)/shard_map/ppermute | solution.py:21
  10.6 3.3 %collective-permute-start.3 = (bf16[128]{0:T(256)(128)(2,1)S(1)}, bf16[128]{0:T(256)(128)(2,1)S(1)}, u32[]{:S(2)}, u32[]{:S(2)}) collective-permute-start(bf16[128]{0:T(256)(128)(2,1)S(1)} %get-tuple-element.16), channel_id=1, source_target_pairs={{2,0},{4,2},{6,4},{8,6},{10,8},{12,10},{14,12},{16,14},{18,16},{20... | collective-permute-start | bytes 776 | tf_op jit(solution)/shard_map/ppermute | solution.py:23
  14.0 0.8 fusion.42
  14.8 2.5 %collective-permute-start.4 = (bf16[128,128]{1,0:T(8,128)(2,1)S(1)}, bf16[128,128]{1,0:T(8,128)(2,1)S(1)}, u32[]{:S(2)}, u32[]{:S(2)}) collective-permute-start(bf16[128,128]{1,0:T(8,128)(2,1)S(1)} %get-tuple-element.11), channel_id=1, source_target_pairs={{0,2},{2,4},{4,6},{6,8},{8,10},{10,12},{12,14},{14,16},{16,18},{18... | collective-permute-start | bytes 98312 | tf_op jit(solution)/shard_map/ppermute | solution.py:21
  17.3 4.2 %collective-permute-start.5 = (bf16[128,128]{1,0:T(8,128)(2,1)S(1)}, bf16[128,128]{1,0:T(8,128)(2,1)S(1)}, u32[]{:S(2)}, u32[]{:S(2)}) collective-permute-start(bf16[128,128]{1,0:T(8,128)(2,1)S(1)} %get-tuple-element.12), channel_id=1, source_target_pairs={{2,0},{4,2},{6,4},{8,6},{10,8},{12,10},{14,12},{16,14},{18,16},{20... | collective-permute-start | bytes 98312 | tf_op jit(solution)/shard_map/ppermute | solution.py:23
  21.5 0.8 fusion.41
  22.3 2.9 %collective-permute-start = (bf16[128,128]{1,0:T(8,128)(2,1)S(1)}, bf16[128,128]{1,0:T(8,128)(2,1)S(1)}, u32[]{:S(2)}, u32[]{:S(2)}) collective-permute-start(bf16[128,128]{1,0:T(8,128)(2,1)S(1)} %get-tuple-element.7), channel_id=1, source_target_pairs={{0,2},{2,4},{4,6},{6,8},{8,10},{10,12},{12,14},{14,16},{16,18},{18... | collective-permute-start | bytes 98312 | tf_op jit(solution)/shard_map/ppermute | solution.py:21
  25.2 0.7 convert_bitcast_fusion
  25.9 0.1 iota_add_fusion
  25.9 0.1 compare_and_fusion
  26.0 0.1 iota_add_fusion.1
  26.1 1.0 reshape.270
  27.1 1.0 copy.18
  28.1 3.9 %collective-permute-start.1 = (bf16[128,128]{1,0:T(8,128)(2,1)S(1)}, bf16[128,128]{1,0:T(8,128)(2,1)S(1)}, u32[]{:S(2)}, u32[]{:S(2)}) collective-permute-start(bf16[128,128]{1,0:T(8,128)(2,1)S(1)} %get-tuple-element.8), channel_id=1, source_target_pairs={{2,0},{4,2},{6,4},{8,6},{10,8},{12,10},{14,12},{16,14},{18,16},{20... | collective-permute-start | bytes 98312 | tf_op jit(solution)/shard_map/ppermute | solution.py:23
  32.0 0.4 fusion.21
  32.4 0.8 pad_maximum_fusion.1
  33.2 0.0 copy-start.3
  33.2 1.3 fusion.8
  34.5 0.1 broadcast_maximum_fusion
  34.6 0.3 fusion.11
  34.9 0.1 exponential_add_fusion
  34.9 0.7 collective-permute-done.1
  35.7 0.1 copy.17
  35.8 0.1 copy.19
  36.0 0.5 fusion.12
  36.5 0.2 copy.22
  36.7 3.7 %fusion.4 = f32[256,2048]{1,0:T(8,128)} fusion(bf16[1024,2048]{1,0:T(8,128)(2,1)} %param.19, s32[]{:T(128)S(6)} %select_n.45, bf16[32,8,4,128]{3,2,1,0:T(4,128)(2,1)S(1)} %bitcast.103), kind=kOutput, calls=%fused_computation.14 | convolution fusion | flops 536870912 | bytes 4456452 | tf_op jit(solution)/shard_map/dot_general | solution.py:105
  40.4 0.0 reduce-scatter.2.cloned.1.call-update
  40.4 0.0 copy-start.1
  40.4 0.0 all-gather.4.cloned.1.call-start
  40.5 0.7 all-gather.4.cloned.1.call-update
  41.2 0.0 all-gather.6.cloned.1.call-start
  41.2 0.7 all-gather.6.cloned.1.call-update
  41.9 0.1 copy.25
  42.1 0.1 eq.49
  42.2 0.1 eq.45
  42.3 0.6 reduce-window.6
  42.9 0.2 slice_reduce_fusion
  43.2 0.1 copy.24
  43.3 0.1 mul.100
  43.5 0.1 fusion.35
  43.6 9.5 %reduce-scatter.2.cloned.1.call-done = f32[128,2048]{1,0:T(8,128)} async-done(((f32[256,2048]{1,0:T(8,128)}), f32[128,2048]{1,0:T(8,128)}) %reduce-scatter.2.cloned.1.call-update) | async-done | bytes 1048592 | tf_op jit(solution)/shard_map/reduce_scatter | solution.py:104
  53.1 1.5 multiply_reduce_fusion.1
  54.7 0.2 multiply_convert_fusion.1
  54.8 7.0 %scatter_custom_fusion = bf16[512,2048]{1,0:T(8,128)(2,1)} fusion(s32[256]{0:T(256)S(1)} %bitcast.110, bf16[128,2048]{1,0:T(8,128)(2,1)S(1)} %multiply_convert_fusion.1, s32[1024]{0:T(1024)S(1)} %pad_clamp_fusion.1, bf16[]{:T(256)} %constant.58.clone.1), kind=kCustom, calls=%fused_computation.26 | custom fusion | bytes 2097154 | tf_op jit(solution)/shard_map/scatter | solution.py:122
  61.9 7.0 %all-to-all-start = ((bf16[16,32,2048]{2,1,0:T(8,128)(2,1)}), bf16[16,32,2048]{2,1,0:T(8,128)(2,1)S(1)}, u32[]{:S(2)}, u32[]{:S(2)}) async-start(bf16[16,32,2048]{2,1,0:T(8,128)(2,1)} %bitcast.25), calls=%async_computation.1 | async-start | bytes 4194304 | tf_op jit(solution)/shard_map/all_to_all | solution.py:123
  68.8 0.2 all-gather.8.cloned.1.call-start
  69.1 0.3 all-gather.8.cloned.1.call-update
  69.4 0.1 all-gather.4.cloned.1.call-done
  69.5 47.7 %all-to-all-done = bf16[16,32,2048]{2,1,0:T(8,128)(2,1)S(1)} async-done(((bf16[16,32,2048]{2,1,0:T(8,128)(2,1)}), bf16[16,32,2048]{2,1,0:T(8,128)(2,1)S(1)}, u32[]{:S(2)}, u32[]{:S(2)}) %all-to-all-start) | async-done | bytes 2097184 | tf_op jit(solution)/shard_map/all_to_all | solution.py:123
  117.2 5.8 %fusion.2 = f32[512,1024]{1,0:T(8,128)} fusion(bf16[512,2048]{1,0:T(8,128)(2,1)S(1)} %bitcast.100, bf16[1,2048,1024]{2,1,0:T(8,128)(2,1)} %all-gather.4.cloned.1.call-done), kind=kOutput, calls=%fused_computation.5 | convolution fusion | flops 2147483648 | bytes 8388608 | tf_op jit(solution)/shard_map/dot_general | solution.py:125
  123.1 6.3 %multiply_convert_fusion = bf16[512,1024]{1,0:T(8,128)(2,1)} fusion(f32[512,1024]{1,0:T(8,128)} %fusion.2, bf16[512,2048]{1,0:T(8,128)(2,1)S(1)} %bitcast.101, bf16[1,2048,1024]{2,1,0:T(8,128)(2,1)} %all-gather.6.cloned.1.call-done), kind=kOutput, calls=%fused_computation.13 | convolution fusion | flops 2150629376 | bytes 9437184 | tf_op jit(solution)/shard_map/dot_general | solution.py:126
  129.4 3.2 %convolution_convert_fusion = bf16[512,2048]{1,0:T(8,128)(2,1)S(1)} fusion(bf16[1,1024,2048]{2,1,0:T(8,128)(2,1)} %all-gather.8.cloned.1.call-done, bf16[512,1024]{1,0:T(8,128)(2,1)} %multiply_convert_fusion), kind=kOutput, calls=%fused_computation.8 | convolution fusion | flops 1074790400 | bytes 4718592 | tf_op jit(solution)/shard_map/dot_general | solution.py:131
  132.5 0.1 copy-done.9
  132.6 2.6 %add_convert_fusion = bf16[512,2048]{1,0:T(8,128)(2,1)} fusion(bf16[512,2048]{1,0:T(8,128)(2,1)S(1)} %convolution_convert_fusion, bf16[1,1024,2048]{2,1,0:T(8,128)(2,1)S(1)} %copy-done.8, bf16[512,1024]{1,0:T(8,128)(2,1)S(1)} %copy-done.9), kind=kOutput, calls=%fused_computation.7 | convolution fusion | flops 1078984704 | bytes 6815744 | tf_op jit(solution)/shard_map/dot_general | solution.py:131
  135.2 5.2 %all-to-all-start.1 = ((bf16[16,32,2048]{2,1,0:T(8,128)(2,1)}), bf16[16,32,2048]{2,1,0:T(8,128)(2,1)S(1)}, u32[]{:S(2)}, u32[]{:S(2)}) async-start(bf16[16,32,2048]{2,1,0:T(8,128)(2,1)} %bitcast.102), calls=%async_computation.2 | async-start | bytes 4194304 | tf_op jit(solution)/shard_map/all_to_all | solution.py:138
  140.5 0.1 copy.23
  140.6 47.6 %all-to-all-done.1 = bf16[16,32,2048]{2,1,0:T(8,128)(2,1)S(1)} async-done(((bf16[16,32,2048]{2,1,0:T(8,128)(2,1)}), bf16[16,32,2048]{2,1,0:T(8,128)(2,1)S(1)}, u32[]{:S(2)}, u32[]{:S(2)}) %all-to-all-start.1) | async-done | bytes 2097184 | tf_op jit(solution)/shard_map/all_to_all | solution.py:138
  188.2 2.3 %gather_fusion = bf16[256,2048]{1,0:T(8,128)(2,1)} fusion(bf16[512,2048]{1,0:T(8,128)(2,1)S(1)} %bitcast.99, s32[1024]{0:T(1024)S(1)} %pad_clamp_fusion), kind=kCustom, calls=%fused_computation.1 | custom fusion | bytes 2098176 | tf_op jit(solution)/shard_map/gather | solution.py:139
  190.5 2.4 %reshape.274 = f32[128,2,2048]{2,1,0:T(2,128)S(1)} reshape(bf16[256,2048]{1,0:T(8,128)(2,1)} %gather_fusion) | data formatting | bytes 3145728 | tf_op jit(solution)/shard_map/convert_element_type | solution.py:139
  192.9 0.0 copy-start.2
  192.9 3.2 %multiply_reduce_fusion = f32[128,2048]{1,0:T(8,128)S(1)} fusion(f32[128,2,2048]{2,1,0:T(2,128)S(1)} %reshape.274, f32[128,2]{1,0:T(8,128)S(1)} %copy.23), kind=kLoop, calls=%fused_computation.12 | loop fusion | flops 786432 | bytes 3146752 | tf_op jit(solution)/shard_map/reduce_sum | solution.py:140
  196.1 1.0 add_convert_fusion.1
  (40 shorter events, 0.2 us)
Async XLA Ops:
  6.5 27.9 %copy-start.6 = (f32[4]{0:T(128)S(1)}, f32[4]{0:T(128)}, u32[]{:S(2)}) copy-start(f32[4]{0:T(128)} %param.18) | copy-start | bytes 52
  6.5 46.6 %reduce-scatter.2.cloned.1.call-start = ((), (), s32[]{:S(2)}) async-start(), calls=%async_computation.3 | async-start | bytes 3145728 | tf_op jit(solution)/shard_map/reduce_scatter | solution.py:104
  7.2 20.8 %collective-permute-start.2 = (bf16[128]{0:T(256)(128)(2,1)S(1)}, bf16[128]{0:T(256)(128)(2,1)S(1)}, u32[]{:S(2)}, u32[]{:S(2)}) collective-permute-start(bf16[128]{0:T(256)(128)(2,1)S(1)} %get-tuple-element.15), channel_id=1, source_target_pairs={{0,2},{2,4},{4,6},{6,8},{8,10},{10,12},{12,14},{14,16},{16,18},{18... | collective-permute-start | bytes 776 | tf_op jit(solution)/shard_map/ppermute | solution.py:21
  10.6 21.3 %collective-permute-start.3 = (bf16[128]{0:T(256)(128)(2,1)S(1)}, bf16[128]{0:T(256)(128)(2,1)S(1)}, u32[]{:S(2)}, u32[]{:S(2)}) collective-permute-start(bf16[128]{0:T(256)(128)(2,1)S(1)} %get-tuple-element.16), channel_id=1, source_target_pairs={{2,0},{4,2},{6,4},{8,6},{10,8},{12,10},{14,12},{16,14},{18,16},{20... | collective-permute-start | bytes 776 | tf_op jit(solution)/shard_map/ppermute | solution.py:23
  14.8 17.6 %collective-permute-start.4 = (bf16[128,128]{1,0:T(8,128)(2,1)S(1)}, bf16[128,128]{1,0:T(8,128)(2,1)S(1)}, u32[]{:S(2)}, u32[]{:S(2)}) collective-permute-start(bf16[128,128]{1,0:T(8,128)(2,1)S(1)} %get-tuple-element.11), channel_id=1, source_target_pairs={{0,2},{2,4},{4,6},{6,8},{8,10},{10,12},{12,14},{14,16},{16,18},{18... | collective-permute-start | bytes 98312 | tf_op jit(solution)/shard_map/ppermute | solution.py:21
  17.3 15.1 %collective-permute-start.5 = (bf16[128,128]{1,0:T(8,128)(2,1)S(1)}, bf16[128,128]{1,0:T(8,128)(2,1)S(1)}, u32[]{:S(2)}, u32[]{:S(2)}) collective-permute-start(bf16[128,128]{1,0:T(8,128)(2,1)S(1)} %get-tuple-element.12), channel_id=1, source_target_pairs={{2,0},{4,2},{6,4},{8,6},{10,8},{12,10},{14,12},{16,14},{18,16},{20... | collective-permute-start | bytes 98312 | tf_op jit(solution)/shard_map/ppermute | solution.py:23
  22.3 12.6 %collective-permute-start = (bf16[128,128]{1,0:T(8,128)(2,1)S(1)}, bf16[128,128]{1,0:T(8,128)(2,1)S(1)}, u32[]{:S(2)}, u32[]{:S(2)}) collective-permute-start(bf16[128,128]{1,0:T(8,128)(2,1)S(1)} %get-tuple-element.7), channel_id=1, source_target_pairs={{0,2},{2,4},{4,6},{6,8},{8,10},{10,12},{12,14},{14,16},{16,18},{18... | collective-permute-start | bytes 98312 | tf_op jit(solution)/shard_map/ppermute | solution.py:21
  28.1 7.6 %collective-permute-start.1 = (bf16[128,128]{1,0:T(8,128)(2,1)S(1)}, bf16[128,128]{1,0:T(8,128)(2,1)S(1)}, u32[]{:S(2)}, u32[]{:S(2)}) collective-permute-start(bf16[128,128]{1,0:T(8,128)(2,1)S(1)} %get-tuple-element.8), channel_id=1, source_target_pairs={{2,0},{4,2},{6,4},{8,6},{10,8},{12,10},{14,12},{16,14},{18,16},{20... | collective-permute-start | bytes 98312 | tf_op jit(solution)/shard_map/ppermute | solution.py:23
  33.2 2.5 %copy-start.3 = (bf16[256,128]{1,0:T(8,128)(2,1)S(1)}, bf16[256,128]{1,0:T(8,128)(2,1)}, u32[]{:S(2)}) copy-start(bf16[256,128]{1,0:T(8,128)(2,1)} %param.16) | copy-start | bytes 196612
  40.4 1.5 copy-start.5
  40.4 12.7 %copy-start.1 = (bf16[128,2048]{1,0:T(8,128)(2,1)S(1)}, bf16[128,2048]{1,0:T(8,128)(2,1)}, u32[]{:S(2)}) copy-start(bf16[128,2048]{1,0:T(8,128)(2,1)} %param.13) | copy-start | bytes 1572868
  40.4 29.1 %all-gather.4.cloned.1.call-start = ((), (), s32[]{:S(2)}) async-start(), calls=%async_computation.4 | async-start | bytes 6291456 | tf_op jit(solution)/shard_map/all_gather | solution.py:59
  41.2 13.5 %copy-start.4 = (f32[2048]{0:T(1024)S(1)}, f32[2048]{0:T(1024)}, u32[]{:S(2)}) copy-start(f32[2048]{0:T(1024)} %param.20) | copy-start | bytes 24580
  41.2 81.9 %all-gather.6.cloned.1.call-start = ((), (), s32[]{:S(2)}) async-start(), calls=%async_computation.5 | async-start | bytes 6291456 | tf_op jit(solution)/shard_map/all_gather | solution.py:60
  53.1 1.6 copy-start
  61.9 55.3 %all-to-all-start = ((bf16[16,32,2048]{2,1,0:T(8,128)(2,1)}), bf16[16,32,2048]{2,1,0:T(8,128)(2,1)S(1)}, u32[]{:S(2)}, u32[]{:S(2)}) async-start(bf16[16,32,2048]{2,1,0:T(8,128)(2,1)} %bitcast.25), calls=%async_computation.1 | async-start | bytes 4194304 | tf_op jit(solution)/shard_map/all_to_all | solution.py:123
  68.8 60.5 %all-gather.8.cloned.1.call-start = ((), (), s32[]{:S(2)}) async-start(), calls=%async_computation.6 | async-start | bytes 6291456 | tf_op jit(solution)/shard_map/all_gather | solution.py:61
  129.4 3.2 %copy-start.8 = (bf16[1,1024,2048]{2,1,0:T(8,128)(2,1)S(1)}, bf16[1,1024,2048]{2,1,0:T(8,128)(2,1)}, u32[]{:S(2)}) copy-start(bf16[1,1024,2048]{2,1,0:T(8,128)(2,1)} %all-gather.8.cloned.1.call-done) | copy-start | bytes 12582916
  129.4 3.3 %copy-start.9 = (bf16[512,1024]{1,0:T(8,128)(2,1)S(1)}, bf16[512,1024]{1,0:T(8,128)(2,1)}, u32[]{:S(2)}) copy-start(bf16[512,1024]{1,0:T(8,128)(2,1)} %multiply_convert_fusion) | copy-start | bytes 3145732
  135.2 5.2 %copy-start.7 = (f32[128,2]{0,1:T(2,128)S(1)}, f32[128,2]{0,1:T(2,128)}, u32[]{:S(2)}) copy-start(f32[128,2]{0,1:T(2,128)} %param.25) | copy-start | bytes 3076
  135.2 52.9 %all-to-all-start.1 = ((bf16[16,32,2048]{2,1,0:T(8,128)(2,1)}), bf16[16,32,2048]{2,1,0:T(8,128)(2,1)S(1)}, u32[]{:S(2)}, u32[]{:S(2)}) async-start(bf16[16,32,2048]{2,1,0:T(8,128)(2,1)} %bitcast.102), calls=%async_computation.2 | async-start | bytes 4194304 | tf_op jit(solution)/shard_map/all_to_all | solution.py:138
  192.9 3.2 %copy-start.2 = (bf16[128,2048]{1,0:T(8,128)(2,1)S(1)}, bf16[128,2048]{1,0:T(8,128)(2,1)}, u32[]{:S(2)}) copy-start(bf16[128,2048]{1,0:T(8,128)(2,1)} %param.13) | copy-start | bytes 1572868
Sparse Core Ops, SparseCore 0:
  40.5 12.5 reduce-scatter.1
  54.6 14.8 all-gather.3
  71.1 14.8 all-gather.5
  87.3 14.8 all-gather.7
where the time goes:
time: 204 us
  waiting for transfers between devices  107 us (52%)
  starting transfers between devices  32.7 us (16%)
  matrix products  23.4 us (11%)
  local copies, waits for them, and re-layouts  16.8 us (8%)
  between operations  13.5 us (7%)
  other arithmetic  9.87 us (5%)
    all_to_all x1, waiting for transfers between devices, local(): lax.all_to_all(outgoing, 'sp', split_axis=0, concat_axis=0, tiled=True)  47.7 us
    all_to_all x1, waiting for transfers between devices, local(): lax.all_to_all(returning, 'sp', split_axis=0, concat_axis=0, tiled=True)  47.6 us
    ppermute x3, starting transfers between devices, with_halo(): lax.ppermute(head, axis, [((i + 1) % count, i) for i in range(ends)])  11.4 us
    reduce_scatter x1, waiting for transfers between devices, local(): lax.psum_scatter(jnp.dot(attended, w_rows, preferred_element_type=jnp.flo...  9.53 us
    ppermute x3, starting transfers between devices, with_halo(): lax.ppermute(tail, axis, [(i, (i + 1) % count) for i in range(ends)])  8.74 us
    scatter x1, local copies, waits for them, and re-layouts, local(): jnp.zeros((n_sp * cap, width_d), jnp.bfloat16).at[slot].set(normed[owner])  7.03 us
    all_to_all x1, starting transfers between devices, local(): lax.all_to_all(outgoing, 'sp', split_axis=0, concat_axis=0, tiled=True)  6.97 us
    dot_general x1, matrix products, local(): jnp.dot(landed, whole_up[0], preferred_element_type=jnp.float32)  6.28 us
  transfers between devices with their start and end apart: 12, of which 5 were waited for; matrix products, arithmetic and copies ran while one was open for 15% of the time, Pallas kernels for 0%

commit v1 on v0

v1 whole, which is shorter than its diff:
```python
import functools

import jax
import jax.numpy as jnp
from jax import lax
from jax.experimental import pallas as pl
from jax.experimental.pallas import tpu as pltpu
from jax.sharding import PartitionSpec as P

HEAD_WIDTH = 128
RADIUS = 128
EPS = 1e-06
MESH = pl.DeviceIdType.MESH
F32 = jnp.float32
BF16 = jnp.bfloat16


def kernel(
    n_sp,
    n_tp,
    cap,
    resid_hbm,
    q_ref,
    k_ref,
    v_ref,
    docs_ref,
    sink_ref,
    wout_hbm,
    gain_ref,
    gate_hbm,
    up_hbm,
    down_hbm,
    ids_ref,
    rw_ref,
    out_ref,
    kext,
    vext,
    dext,
    gbuf,
    ubuf,
    dbuf,
    wobuf,
    resid,
    att,
    attsend,
    mixed,
    outgoing,
    landed,
    ret,
    back,
    halo_send,
    halo_recv,
    w_send,
    w_recv,
    loc_sem,
    att_send_sem,
    att_recv_sem,
    d_send,
    d_recv,
    r_send,
    r_recv,
):
    sp = lax.axis_index("sp")
    tp = lax.axis_index("tp")
    other = n_tp - 1 - tp
    rows_all = q_ref.shape[0]
    heads = q_ref.shape[1] // HEAD_WIDTH
    nb = rows_all // RADIUS
    keep = rows_all // n_tp
    width = q_ref.shape[1]
    dim = out_ref.shape[1]
    total_pos = n_sp * rows_all

    barrier = pltpu.get_barrier_semaphore()

    @pl.loop(1, n_sp)
    def _(o):
        pl.semaphore_signal(
            barrier, inc=1, device_id=(lax.rem(sp + o, n_sp), tp), device_id_type=MESH
        )

    pl.semaphore_signal(barrier, inc=1, device_id=(sp, other), device_id_type=MESH)

    local_copies = [
        pltpu.make_async_copy(wout_hbm, wobuf, loc_sem.at[0]),
        pltpu.make_async_copy(resid_hbm, resid, loc_sem.at[1]),
        pltpu.make_async_copy(gate_hbm.at[0], gbuf.at[tp], loc_sem.at[2]),
        pltpu.make_async_copy(up_hbm.at[0], ubuf.at[tp], loc_sem.at[3]),
        pltpu.make_async_copy(down_hbm.at[0], dbuf.at[tp], loc_sem.at[4]),
    ]
    for c in local_copies[:2]:
        c.start()

    pl.semaphore_wait(barrier, n_sp)

    right = (lax.rem(sp + 1, n_sp), tp)
    left = (lax.rem(sp + n_sp - 1, n_sp), tp)
    tail = rows_all - RADIUS
    end = rows_all + RADIUS

    def remote(src, dst, s, r, dev):
        return pltpu.make_async_remote_copy(
            src_ref=src, dst_ref=dst, send_sem=s, recv_sem=r, device_id=dev, device_id_type=MESH
        )

    halo = []
    for i, (src, dst) in enumerate(((k_ref, kext), (v_ref, vext))):
        halo.append(
            remote(
                src.at[pl.ds(tail, RADIUS)],
                dst.at[pl.ds(0, RADIUS)],
                halo_send.at[2 * i],
                halo_recv.at[2 * i],
                right,
            )
        )
        halo.append(
            remote(
                src.at[pl.ds(0, RADIUS)],
                dst.at[pl.ds(end, RADIUS)],
                halo_send.at[2 * i + 1],
                halo_recv.at[2 * i + 1],
                left,
            )
        )
    halo.append(
        remote(docs_ref.at[nb - 1], dext.at[0], halo_send.at[4], halo_recv.at[4], right)
    )
    halo.append(
        remote(docs_ref.at[0], dext.at[nb + 1], halo_send.at[5], halo_recv.at[5], left)
    )
    for c in halo:
        c.start()
    partner = (sp, other)
    weights = [
        remote(gate_hbm.at[0], gbuf.at[tp], w_send.at[0], w_recv.at[0], partner),
        remote(up_hbm.at[0], ubuf.at[tp], w_send.at[1], w_recv.at[1], partner),
        remote(down_hbm.at[0], dbuf.at[tp], w_send.at[2], w_recv.at[2], partner),
    ]
    for c in weights:
        c.start()
    for c in local_copies[2:]:
        c.start()

    kext[RADIUS:end, :] = k_ref[...]
    vext[RADIUS:end, :] = v_ref[...]
    for b in range(nb):
        dext[b + 1] = docs_ref[b]

    me = sp
    top_k = ids_ref.shape[1]
    n_slots = n_sp * cap
    lane = lax.broadcasted_iota(jnp.int32, (keep, n_sp), 1)
    hots = [(ids_ref[:, k : k + 1] == lane).astype(F32) for k in range(top_k)]
    visits = sum(hots)
    lower = (
        lax.broadcasted_iota(jnp.int32, (keep, keep), 1)
        < lax.broadcasted_iota(jnp.int32, (keep, keep), 0)
    ).astype(BF16)
    before = jnp.dot(lower, visits.astype(BF16), preferred_element_type=F32)
    slot_lane = lax.broadcasted_iota(jnp.int32, (keep, n_slots), 1).astype(F32)
    picks = []
    for k in range(top_k):
        rank = jnp.sum(hots[k] * before, axis=1, keepdims=True)
        rel = ids_ref[:, k : k + 1] - me
        rel = jnp.where(rel < 0, rel + n_sp, rel)
        slot = rel.astype(F32) * float(cap) + rank
        picks.append((slot == slot_lane).astype(BF16))

    for c in halo:
        c.wait()

    eye = lax.broadcasted_iota(jnp.int32, (RADIUS, RADIUS), 0) == lax.broadcasted_iota(
        jnp.int32, (RADIUS, RADIUS), 1
    )

    def attend(b):
        row0 = pl.multiple_of(b * RADIUS, RADIUS)
        keys = kext[pl.ds(row0, 3 * RADIUS), :]
        vals = vext[pl.ds(row0, 3 * RADIUS), :]
        kdoc = jnp.concatenate([dext[b], dext[b + 1], dext[b + 2]], axis=1)
        qdoc = jnp.sum(
            jnp.where(eye, jnp.broadcast_to(dext[b + 1], (RADIUS, RADIUS)), 0).astype(F32),
            axis=1,
            keepdims=True,
        )
        qi = lax.broadcasted_iota(jnp.int32, (RADIUS, 3 * RADIUS), 0)
        kj = lax.broadcasted_iota(jnp.int32, (RADIUS, 3 * RADIUS), 1)
        where_key = kj + (sp * rows_all + (b - 1) * RADIUS)
        valid = (
            (kj >= qi)
            & (kj <= qi + 2 * RADIUS)
            & (where_key >= 0)
            & (where_key < total_pos)
            & (kdoc.astype(F32) == qdoc)
        )
        parts = []
        for h in range(heads):
            qh = q_ref[pl.ds(row0, RADIUS), h * HEAD_WIDTH : (h + 1) * HEAD_WIDTH]
            s = lax.dot_general(
                qh, keys, (((1,), (1,)), ((), ())), preferred_element_type=F32
            ) * (HEAD_WIDTH**-0.5)
            sk = sink_ref[:, h : h + 1]
            s = jnp.where(valid, s, -jnp.inf)
            top = jnp.maximum(jnp.max(s, axis=1, keepdims=True), sk)
            e = jnp.exp(s - top)
            den = jnp.sum(e, axis=1, keepdims=True) + jnp.exp(sk - top)
            p = (e * (1.0 / den)).astype(BF16)
            parts.append(jnp.dot(p, vals, preferred_element_type=F32).astype(BF16))
        return jnp.concatenate(parts, axis=1)

    attsend[...] = attend(other)
    att_copy = remote(attsend, att.at[tp], att_send_sem, att_recv_sem, partner)
    att_copy.start()
    att[tp] = attend(tp)

    for c in local_copies[:2]:
        c.wait()

    def project(p):
        w = wobuf[pl.ds(pl.multiple_of(p * width, width), width), :]
        return jnp.dot(att[p], w, preferred_element_type=F32)

    mixed[...] = resid[...].astype(F32) + project(tp)
    att_copy.wait()
    mx = mixed[...] + project(other)
    mixed[...] = mx
    scale = lax.rsqrt(jnp.mean(mx * mx, axis=1, keepdims=True) + EPS)
    normed = (mx * scale * gain_ref[...]).astype(BF16)
    spread = (picks[0] + picks[1]) if top_k == 2 else sum(picks)
    outgoing[...] = lax.dot_general(
        spread, normed, (((0,), (0,)), ((), ())), preferred_element_type=F32
    ).astype(BF16)

    def block(o):
        return pl.ds(pl.multiple_of(o * cap, cap), cap)

    def disp(o):
        return remote(
            outgoing.at[block(o)],
            landed.at[block(o)],
            d_send.at[o],
            d_recv.at[o],
            (lax.rem(sp + o, n_sp), tp),
        )

    def home(o):
        return remote(
            ret.at[block(o)],
            back.at[block(o)],
            r_send.at[o],
            r_recv.at[o],
            (lax.rem(sp + n_sp - o, n_sp), tp),
        )

    @pl.loop(1, n_sp)
    def _(o):
        disp(o).start()

    landed[0:cap, :] = outgoing[0:cap, :]

    for c in local_copies[2:]:
        c.wait()
    for c in weights:
        c.wait()

    group = max(1, min(n_sp, 128 // cap))
    grows = group * cap

    @pl.loop(0, n_sp // group)
    def _(g):
        @pl.loop(0, group)
        def _(i):
            @pl.when(g * group + i > 0)
            def _():
                disp(g * group + i).wait_recv()

        rows = pl.ds(pl.multiple_of(g * grows, grows), grows)
        x = landed[rows, :]
        acc = jnp.zeros((grows, dim), F32)
        for p in range(n_tp):
            a = jnp.dot(x, gbuf[p], preferred_element_type=F32)
            u = jnp.dot(x, ubuf[p], preferred_element_type=F32)
            hid = (a * jax.nn.sigmoid(a) * u).astype(BF16)
            part = jnp.dot(hid, dbuf[p], preferred_element_type=F32).astype(BF16)
            acc = acc + part.astype(F32)
        ret[rows, :] = acc.astype(BF16)

        @pl.loop(0, group)
        def _(i):
            @pl.when(g * group + i > 0)
            def _():
                home(g * group + i).start()

    back[0:cap, :] = ret[0:cap, :]
    w0 = rw_ref[:, 0:1]
    w1 = rw_ref[:, 1:2]
    for g in range(n_sp // group):

        @pl.loop(max(1, g * group), (g + 1) * group)
        def _(o):
            home(o).wait_recv()

        sl = slice(g * grows, (g + 1) * grows)
        chunk = back[sl, :]
        mixed[...] += w0 * jnp.dot(
            picks[0][:, sl], chunk, preferred_element_type=F32
        ) + w1 * jnp.dot(picks[1][:, sl], chunk, preferred_element_type=F32)
    out_ref[...] = mixed[...].astype(BF16)

    @pl.loop(1, n_sp)
    def _(o):
        disp(o).wait_send()
        home(o).wait_send()


def local(n_sp, n_tp, *args):
    (resid, queries, keys, values, docs, sink, w_out, gain, w_gate, w_up, w_down, ids, rw) = args
    rows_all = queries.shape[0]
    keep, dim = resid.shape
    top_k = ids.shape[1]
    cap = max(16, rows_all * top_k // n_sp)
    nb = rows_all // RADIUS
    ff = w_gate.shape[2]
    slots = n_sp * cap
    vm = pl.BlockSpec(memory_space=pltpu.VMEM)
    hbm = pl.BlockSpec(memory_space=pl.ANY)
    dma = pltpu.SemaphoreType.DMA
    return pl.pallas_call(
        functools.partial(kernel, n_sp, n_tp, cap),
        out_shape=jax.ShapeDtypeStruct((keep, dim), BF16),
        in_specs=[hbm, vm, vm, vm, vm, vm, hbm, vm, hbm, hbm, hbm, vm, vm],
        out_specs=vm,
        scratch_shapes=[
            pltpu.VMEM((rows_all + 2 * RADIUS, keys.shape[1]), BF16),
            pltpu.VMEM((rows_all + 2 * RADIUS, keys.shape[1]), BF16),
            pltpu.VMEM((nb + 2, 1, RADIUS), jnp.int32),
            pltpu.VMEM((n_tp, dim, ff), BF16),
            pltpu.VMEM((n_tp, dim, ff), BF16),
            pltpu.VMEM((n_tp, ff, dim), BF16),
            pltpu.VMEM(w_out.shape, BF16),
            pltpu.VMEM((keep, dim), BF16),
            pltpu.VMEM((n_tp, keep, queries.shape[1]), BF16),
            pltpu.VMEM((keep, queries.shape[1]), BF16),
            pltpu.VMEM((keep, dim), F32),
            pltpu.VMEM((slots, dim), BF16),
            pltpu.VMEM((slots, dim), BF16),
            pltpu.VMEM((slots, dim), BF16),
            pltpu.VMEM((slots, dim), BF16),
            dma((6,)),
            dma((6,)),
            dma((3,)),
            dma((3,)),
            dma((5,)),
            dma,
            dma,
            dma((n_sp,)),
            dma((n_sp,)),
            dma((n_sp,)),
            dma((n_sp,)),
        ],
        compiler_params=pltpu.CompilerParams(
            collective_id=0, has_side_effects=True, vmem_limit_bytes=60 * 1024 * 1024
        ),
    )(
        resid,
        queries,
        keys,
        values,
        docs.reshape(nb, 1, RADIUS),
        sink.reshape(1, -1),
        w_out,
        gain.reshape(1, -1),
        w_gate,
        w_up,
        w_down,
        ids,
        rw,
    )


def solution(mesh):
    in_specs = (
        P(("sp", "tp"), None),
        P("sp", "tp"),
        P("sp", "tp"),
        P("sp", "tp"),
        P("sp"),
        P("tp"),
        P(),
        P(),
        P("sp", None, "tp"),
        P("sp", None, "tp"),
        P("sp", "tp", None),
        P(("sp", "tp"), None),
        P(("sp", "tp"), None),
    )
    return jax.shard_map(
        functools.partial(local, mesh.shape["sp"], mesh.shape["tp"]),
        mesh=mesh,
        in_specs=in_specs,
        out_specs=P(("sp", "tp"), None),
        check_vma=False,
    )
```

time: 204 us -> 133 us (0.65)
  the two profiles are of different devices: /device:TPU:12 before, /device:TPU:0 now
where the time goes in v1:
time: 133 us
  Pallas kernels  128 us (96%)
  local copies, waits for them, and re-layouts  4.7 us (4%)
    pallas_call x1, Pallas kernels, local(): pl.pallas_call(functools.partial(kernel, n_sp, n_tp, cap), out_shape=jax....  128 us
    unnamed x3, local copies, waits for them, and re-layouts  4.7 us

profile of v1, /device:TPU:0, one launch (start us, length us, event | category | flops | bytes accessed | tf_op | source)
XLA Modules:
  0.0 132.6 jit_solution(3391702706971374740)
XLA Ops:
  0.0 1.4 %copy.14.ids_ref = s32[128,2]{1,0:T(8,128)} copy(s32[128,2]{0,1:T(2,128)} %param.24) | data formatting | bytes 2048 | tf_op args[11]
  1.4 1.4 %copy.15.rw_ref = f32[128,2]{1,0:T(8,128)} copy(f32[128,2]{0,1:T(2,128)} %param.25) | data formatting | bytes 2048 | tf_op args[12]
  2.8 127.9 %shard_map.127 = bf16[128,2048]{1,0:T(8,128)(2,1)} custom-call(bf16[128,2048]{1,0:T(8,128)(2,1)} %resid_hbm.1, bf16[256,512]{1,0:T(8,128)(2,1)} %q_ref.1, bf16[256,128]{1,0:T(8,128)(2,1)} %k_ref.1, bf16[256,128]{1,0:T(8,128)(2,1)} %v_ref.1, s32[2,1,128]{2,1,0:T(1,128)} %bitcast.4, f32[1,4]{1,0:T(1,128)} %bitcast.5, bf16[1024,2048]{1,0:T(8,128)(2,1)} %wout_hbm.1, ...), custom_call_target="tpu_custom_call" | custom-call | tf_op jit(solution)/shard_map/pallas_call | solution.py:329
  130.7 1.9 %copy.17 = bf16[128,2048]{1,0:T(8,128)(2,1)} copy(bf16[128,2048]{1,0:T(8,128)(2,1)} %shard_map.127) | data formatting | bytes 1048576

commit v2 on v1

--- a/solution.py
+++ b/solution.py
@@ -19,6 +19,7 @@
     n_sp,
     n_tp,
     cap,
+    parts,
     resid_hbm,
     q_ref,
     k_ref,
@@ -59,6 +60,22 @@
     d_recv,
     r_send,
     r_recv,
+    e_send,
+    e_recv,
+    s_send,
+    s_recv,
+    x_send,
+    x_recv,
+    y_send,
+    y_recv,
+    i_send,
+    i_recv,
+    pids,
+    prw,
+    normed,
+    pnormed,
+    psum,
+    got,
 ):
     sp = lax.axis_index("sp")
     tp = lax.axis_index("tp")
@@ -132,6 +149,13 @@
     for c in halo:
         c.start()
     partner = (sp, other)
+    peer = (lax.rem(sp + n_sp // 2, n_sp), tp)
+    small = [
+        remote(ids_ref, pids, i_send.at[0], i_recv.at[0], peer),
+        remote(rw_ref, prw, i_send.at[1], i_recv.at[1], peer),
+    ]
+    for c in small:
+        c.start()
     weights = [
         remote(gate_hbm.at[0], gbuf.at[tp], w_send.at[0], w_recv.at[0], partner),
         remote(up_hbm.at[0], ubuf.at[tp], w_send.at[1], w_recv.at[1], partner),
@@ -147,25 +171,33 @@
     for b in range(nb):
         dext[b + 1] = docs_ref[b]
 
-    me = sp
+    half = n_sp // 2
+    base = (sp // half) * half
+    mine = lax.rem(sp, half)
     top_k = ids_ref.shape[1]
-    n_slots = n_sp * cap
+    n_slots = half * cap
     lane = lax.broadcasted_iota(jnp.int32, (keep, n_sp), 1)
-    hots = [(ids_ref[:, k : k + 1] == lane).astype(F32) for k in range(top_k)]
-    visits = sum(hots)
     lower = (
         lax.broadcasted_iota(jnp.int32, (keep, keep), 1)
         < lax.broadcasted_iota(jnp.int32, (keep, keep), 0)
     ).astype(BF16)
-    before = jnp.dot(lower, visits.astype(BF16), preferred_element_type=F32)
     slot_lane = lax.broadcasted_iota(jnp.int32, (keep, n_slots), 1).astype(F32)
-    picks = []
-    for k in range(top_k):
-        rank = jnp.sum(hots[k] * before, axis=1, keepdims=True)
-        rel = ids_ref[:, k : k + 1] - me
-        rel = jnp.where(rel < 0, rel + n_sp, rel)
-        slot = rel.astype(F32) * float(cap) + rank
-        picks.append((slot == slot_lane).astype(BF16))
+
+    def route(ref):
+        hots = [(ref[:, k : k + 1] == lane).astype(F32) for k in range(top_k)]
+        before = jnp.dot(lower, sum(hots).astype(BF16), preferred_element_type=F32)
+        picks = []
+        for k in range(top_k):
+            rank = jnp.sum(hots[k] * before, axis=1, keepdims=True)
+            at = ref[:, k : k + 1] - base
+            here = (at >= 0) & (at < half)
+            rel = at - mine
+            rel = jnp.where(rel < 0, rel + half, rel)
+            slot = jnp.where(here, rel.astype(F32) * float(cap) + rank, -1.0)
+            picks.append((slot == slot_lane).astype(BF16))
+        return picks
+
+    picks = route(ids_ref)
 
     for c in halo:
         c.wait()
@@ -226,58 +258,83 @@
     mx = mixed[...] + project(other)
     mixed[...] = mx
     scale = lax.rsqrt(jnp.mean(mx * mx, axis=1, keepdims=True) + EPS)
-    normed = (mx * scale * gain_ref[...]).astype(BF16)
-    spread = (picks[0] + picks[1]) if top_k == 2 else sum(picks)
-    outgoing[...] = lax.dot_general(
-        spread, normed, (((0,), (0,)), ((), ())), preferred_element_type=F32
-    ).astype(BF16)
-
-    def block(o):
-        return pl.ds(pl.multiple_of(o * cap, cap), cap)
+    normed[...] = (mx * scale * gain_ref[...]).astype(BF16)
+    wide = dim // parts
+
+    def cols(c):
+        return pl.ds(c * wide, wide)
+
+    swaps = [
+        remote(
+            normed.at[:, cols(c)], pnormed.at[:, cols(c)], x_send.at[c], x_recv.at[c], peer
+        )
+        for c in range(parts)
+    ]
+    for c in swaps:
+        c.start()
+
+    def spread(chosen, rows):
+        return lax.dot_general(
+            sum(chosen), rows, (((0,), (0,)), ((), ())), preferred_element_type=F32
+        ).astype(BF16)
+
+    def block(o, first=0):
+        return pl.ds(pl.multiple_of(first + o * cap, cap), cap)
+
+    def to(o):
+        return (base + lax.rem(mine + o, half), tp)
+
+    def fro(o):
+        return (base + lax.rem(mine + half - o, half), tp)
 
     def disp(o):
         return remote(
-            outgoing.at[block(o)],
-            landed.at[block(o)],
-            d_send.at[o],
-            d_recv.at[o],
-            (lax.rem(sp + o, n_sp), tp),
+            outgoing.at[block(o)], landed.at[block(o)], d_send.at[o], d_recv.at[o], to(o)
         )
 
     def home(o):
-        return remote(
-            ret.at[block(o)],
-            back.at[block(o)],
-            r_send.at[o],
-            r_recv.at[o],
-            (lax.rem(sp + n_sp - o, n_sp), tp),
-        )
-
-    @pl.loop(1, n_sp)
+        return remote(ret.at[block(o)], back.at[block(o)], r_send.at[o], r_recv.at[o], fro(o))
+
+    def disp2(o, c):
+        sl = (block(o, n_slots), cols(c))
+        i = c * half + o
+        return remote(outgoing.at[sl], landed.at[sl], e_send.at[i], e_recv.at[i], to(o))
+
+    def home2(o, c):
+        sl = (block(o, n_slots), cols(c))
+        i = c * half + o
+        return remote(ret.at[sl], back.at[sl], s_send.at[i], s_recv.at[i], fro(o))
+
+    outgoing[0:n_slots, :] = spread(picks, normed[...])
+
+    @pl.loop(1, half)
     def _(o):
         disp(o).start()
 
     landed[0:cap, :] = outgoing[0:cap, :]
+
+    for c in small:
+        c.wait()
+    ppicks = route(pids)
+    for c in range(parts):
+        swaps[c].wait_recv()
+        cs = slice(c * wide, (c + 1) * wide)
+        outgoing[n_slots : 2 * n_slots, cs] = spread(ppicks, pnormed[:, cs])
+
+        @pl.loop(1, half)
+        def _(o):
+            disp2(o, c).start()
+
+    landed[n_slots : n_slots + cap, :] = outgoing[n_slots : n_slots + cap, :]
 
     for c in local_copies[2:]:
         c.wait()
     for c in weights:
         c.wait()
 
-    group = max(1, min(n_sp, 128 // cap))
-    grows = group * cap
-
-    @pl.loop(0, n_sp // group)
-    def _(g):
-        @pl.loop(0, group)
-        def _(i):
-            @pl.when(g * group + i > 0)
-            def _():
-                disp(g * group + i).wait_recv()
-
-        rows = pl.ds(pl.multiple_of(g * grows, grows), grows)
+    def experts(rows, count):
         x = landed[rows, :]
-        acc = jnp.zeros((grows, dim), F32)
+        acc = jnp.zeros((count, dim), F32)
         for p in range(n_tp):
             a = jnp.dot(x, gbuf[p], preferred_element_type=F32)
             u = jnp.dot(x, ubuf[p], preferred_element_type=F32)
@@ -286,32 +343,84 @@
             acc = acc + part.astype(F32)
         ret[rows, :] = acc.astype(BF16)
 
+    @pl.loop(1, half)
+    def _(o):
+        disp(o).wait_recv()
+
+    experts(slice(0, n_slots), n_slots)
+
+    @pl.loop(1, half)
+    def _(o):
+        home(o).start()
+
+    back[0:cap, :] = ret[0:cap, :]
+
+    group = max(1, min(half, 128 // cap))
+    grows = group * cap
+
+    @pl.loop(0, half // group)
+    def _(g):
         @pl.loop(0, group)
         def _(i):
             @pl.when(g * group + i > 0)
             def _():
-                home(g * group + i).start()
-
-    back[0:cap, :] = ret[0:cap, :]
-    w0 = rw_ref[:, 0:1]
-    w1 = rw_ref[:, 1:2]
-    for g in range(n_sp // group):
-
-        @pl.loop(max(1, g * group), (g + 1) * group)
+                for c in range(parts):
+                    disp2(g * group + i, c).wait_recv()
+
+        experts(pl.ds(pl.multiple_of(n_slots + g * grows, grows), grows), grows)
+
+        for c in range(parts):
+
+            @pl.loop(0, group)
+            def _(i):
+                @pl.when(g * group + i > 0)
+                def _():
+                    home2(g * group + i, c).start()
+
+    back[n_slots : n_slots + cap, :] = ret[n_slots : n_slots + cap, :]
+
+    def gathered(chosen, weight_ref, first, cs):
+        chunk = back[first : first + n_slots, cs]
+        return sum(
+            weight_ref[:, k : k + 1] * jnp.dot(chosen[k], chunk, preferred_element_type=F32)
+            for k in range(top_k)
+        )
+
+    crossings = [
+        remote(psum.at[:, cols(c)], got.at[:, cols(c)], y_send.at[c], y_recv.at[c], peer)
+        for c in range(parts)
+    ]
+    for c in range(parts):
+
+        @pl.loop(1, half)
         def _(o):
-            home(o).wait_recv()
-
-        sl = slice(g * grows, (g + 1) * grows)
-        chunk = back[sl, :]
-        mixed[...] += w0 * jnp.dot(
-            picks[0][:, sl], chunk, preferred_element_type=F32
-        ) + w1 * jnp.dot(picks[1][:, sl], chunk, preferred_element_type=F32)
-    out_ref[...] = mixed[...].astype(BF16)
-
-    @pl.loop(1, n_sp)
+            home2(o, c).wait_recv()
+
+        cs = slice(c * wide, (c + 1) * wide)
+        psum[:, cs] = gathered(ppicks, prw, n_slots, cs).astype(BF16)
+        crossings[c].start()
+
+    @pl.loop(1, half)
+    def _(o):
+        home(o).wait_recv()
+
+    mixed[...] += gathered(picks, rw_ref, 0, slice(0, dim))
+    for c in range(parts):
+        crossings[c].wait_recv()
+        cs = slice(c * wide, (c + 1) * wide)
+        out_ref[:, cs] = (mixed[:, cs] + got[:, cs].astype(F32)).astype(BF16)
+
+    for c in range(parts):
+        swaps[c].wait_send()
+        crossings[c].wait_send()
+
+    @pl.loop(1, half)
     def _(o):
         disp(o).wait_send()
         home(o).wait_send()
+        for c in range(parts):
+            disp2(o, c).wait_send()
+            home2(o, c).wait_send()
 
 
 def local(n_sp, n_tp, *args):
@@ -321,13 +430,15 @@
     top_k = ids.shape[1]
     cap = max(16, rows_all * top_k // n_sp)
     nb = rows_all // RADIUS
+    parts = 2
+    half = n_sp // 2
     ff = w_gate.shape[2]
     slots = n_sp * cap
     vm = pl.BlockSpec(memory_space=pltpu.VMEM)
     hbm = pl.BlockSpec(memory_space=pl.ANY)
     dma = pltpu.SemaphoreType.DMA
     return pl.pallas_call(
-        functools.partial(kernel, n_sp, n_tp, cap),
+        functools.partial(kernel, n_sp, n_tp, cap, parts),
         out_shape=jax.ShapeDtypeStruct((keep, dim), BF16),
         in_specs=[hbm, vm, vm, vm, vm, vm, hbm, vm, hbm, hbm, hbm, vm, vm],
         out_specs=vm,
@@ -354,10 +465,26 @@
             dma((5,)),
             dma,
             dma,
-            dma((n_sp,)),
-            dma((n_sp,)),
-            dma((n_sp,)),
-            dma((n_sp,)),
+            dma((half,)),
+            dma((half,)),
+            dma((half,)),
+            dma((half,)),
+            dma((parts * half,)),
+            dma((parts * half,)),
+            dma((parts * half,)),
+            dma((parts * half,)),
+            dma((parts,)),
+            dma((parts,)),
+            dma((parts,)),
+            dma((parts,)),
+            dma((2,)),
+            dma((2,)),
+            pltpu.VMEM(ids.shape, jnp.int32),
+            pltpu.VMEM(rw.shape, F32),
+            pltpu.VMEM((keep, dim), BF16),
+            pltpu.VMEM((keep, dim), BF16),
+            pltpu.VMEM((keep, dim), BF16),
+            pltpu.VMEM((keep, dim), BF16),
         ],
         compiler_params=pltpu.CompilerParams(
             collective_id=0, has_side_effects=True, vmem_limit_bytes=60 * 1024 * 1024

time: 133 us -> 112 us (0.84)
  Pallas kernels: 128 us -> 107 us
    pallas_call x1, Pallas kernels: 128 us -> 107 us  [local(): pl.pallas_call(functools.partial(kernel, n_sp, n_tp, cap, parts), out_sha...]
where the time goes in v2:
time: 112 us
  Pallas kernels  107 us (96%)
  local copies, waits for them, and re-layouts  4.7 us (4%)
    pallas_call x1, Pallas kernels, local(): pl.pallas_call(functools.partial(kernel, n_sp, n_tp, cap, parts), out_sha...  107 us
    unnamed x3, local copies, waits for them, and re-layouts  4.7 us

profile of v2, /device:TPU:0, one launch (start us, length us, event | category | flops | bytes accessed | tf_op | source)
XLA Modules:
  0.0 111.8 jit_solution(5322502141507117623)
XLA Ops:
  0.0 1.4 %copy.14.ids_ref = s32[128,2]{1,0:T(8,128)} copy(s32[128,2]{0,1:T(2,128)} %param.24) | data formatting | bytes 2048 | tf_op args[11]
  1.4 1.4 %copy.15.rw_ref = f32[128,2]{1,0:T(8,128)} copy(f32[128,2]{0,1:T(2,128)} %param.25) | data formatting | bytes 2048 | tf_op args[12]
  2.8 107.1 %shard_map.127 = bf16[128,2048]{1,0:T(8,128)(2,1)} custom-call(bf16[128,2048]{1,0:T(8,128)(2,1)} %resid_hbm.1, bf16[256,512]{1,0:T(8,128)(2,1)} %q_ref.1, bf16[256,128]{1,0:T(8,128)(2,1)} %k_ref.1, bf16[256,128]{1,0:T(8,128)(2,1)} %v_ref.1, s32[2,1,128]{2,1,0:T(1,128)} %bitcast.4, f32[1,4]{1,0:T(1,128)} %bitcast.5, bf16[1024,2048]{1,0:T(8,128)(2,1)} %wout_hbm.1, ...), custom_call_target="tpu_custom_call" | custom-call | tf_op jit(solution)/shard_map/pallas_call | solution.py:440
  109.9 1.9 %copy.17 = bf16[128,2048]{1,0:T(8,128)(2,1)} copy(bf16[128,2048]{1,0:T(8,128)(2,1)} %shard_map.127) | data formatting | bytes 1048576

commit v3 on v2

--- a/solution.py
+++ b/solution.py
@@ -90,13 +90,31 @@
 
     barrier = pltpu.get_barrier_semaphore()
 
-    @pl.loop(1, n_sp)
+    half = n_sp // 2
+    base = (sp // half) * half
+    mine = lax.rem(sp, half)
+    partner = (sp, other)
+    peer = (lax.rem(sp + half, n_sp), tp)
+    right = (lax.rem(sp + 1, n_sp), tp)
+    left = (lax.rem(sp + n_sp - 1, n_sp), tp)
+
+    def hello(dev):
+        pl.semaphore_signal(barrier, inc=1, device_id=dev, device_id_type=MESH)
+
+    def if_left(f):
+        pl.when(sp > 0)(f)
+
+    def if_right(f):
+        pl.when(sp < n_sp - 1)(f)
+
+    hello(peer)
+    if_left(lambda: hello(left))
+    if_right(lambda: hello(right))
+    hello(partner)
+
+    @pl.loop(1, half)
     def _(o):
-        pl.semaphore_signal(
-            barrier, inc=1, device_id=(lax.rem(sp + o, n_sp), tp), device_id_type=MESH
-        )
-
-    pl.semaphore_signal(barrier, inc=1, device_id=(sp, other), device_id_type=MESH)
+        hello((base + lax.rem(mine + o, half), tp))
 
     local_copies = [
         pltpu.make_async_copy(wout_hbm, wobuf, loc_sem.at[0]),
@@ -108,12 +126,28 @@
     for c in local_copies[:2]:
         c.start()
 
-    pl.semaphore_wait(barrier, n_sp)
-
-    right = (lax.rem(sp + 1, n_sp), tp)
-    left = (lax.rem(sp + n_sp - 1, n_sp), tp)
     tail = rows_all - RADIUS
     end = rows_all + RADIUS
+    kext[RADIUS:end, :] = k_ref[...]
+    vext[RADIUS:end, :] = v_ref[...]
+    for b in range(nb):
+        dext[b + 1] = docs_ref[b]
+
+    def blank(row, b):
+        def fill():
+            zero = jnp.zeros((RADIUS, kext.shape[1]), BF16)
+            kext[row : row + RADIUS, :] = zero
+            vext[row : row + RADIUS, :] = zero
+            dext[b] = jnp.zeros((1, RADIUS), jnp.int32)
+
+        return fill
+
+    pl.when(sp == 0)(blank(0, 0))
+    pl.when(sp == n_sp - 1)(blank(end, nb + 1))
+
+    has_left = (sp + n_sp - 1) // n_sp
+    has_right = (2 * n_sp - 2 - sp) // n_sp
+    pl.semaphore_wait(barrier, half + 1 + has_left + has_right)
 
     def remote(src, dst, s, r, dev):
         return pltpu.make_async_remote_copy(
@@ -146,10 +180,9 @@
     halo.append(
         remote(docs_ref.at[0], dext.at[nb + 1], halo_send.at[5], halo_recv.at[5], left)
     )
-    for c in halo:
-        c.start()
-    partner = (sp, other)
-    peer = (lax.rem(sp + n_sp // 2, n_sp), tp)
+    for i in range(0, len(halo), 2):
+        if_right(halo[i].start)
+        if_left(halo[i + 1].start)
     small = [
         remote(ids_ref, pids, i_send.at[0], i_recv.at[0], peer),
         remote(rw_ref, prw, i_send.at[1], i_recv.at[1], peer),
@@ -161,46 +194,46 @@
         remote(up_hbm.at[0], ubuf.at[tp], w_send.at[1], w_recv.at[1], partner),
         remote(down_hbm.at[0], dbuf.at[tp], w_send.at[2], w_recv.at[2], partner),
     ]
-    for c in weights:
-        c.start()
-    for c in local_copies[2:]:
-        c.start()
-
-    kext[RADIUS:end, :] = k_ref[...]
-    vext[RADIUS:end, :] = v_ref[...]
-    for b in range(nb):
-        dext[b + 1] = docs_ref[b]
-
-    half = n_sp // 2
-    base = (sp // half) * half
-    mine = lax.rem(sp, half)
-    top_k = ids_ref.shape[1]
+
+    top_k = ids_ref.shape[0]
     n_slots = half * cap
-    lane = lax.broadcasted_iota(jnp.int32, (keep, n_sp), 1)
+    lane = lax.broadcasted_iota(jnp.int32, (keep, n_sp), 1).astype(F32)
+    base_f = base.astype(F32)
+    mine_f = mine.astype(F32)
     lower = (
         lax.broadcasted_iota(jnp.int32, (keep, keep), 1)
         < lax.broadcasted_iota(jnp.int32, (keep, keep), 0)
     ).astype(BF16)
     slot_lane = lax.broadcasted_iota(jnp.int32, (keep, n_slots), 1).astype(F32)
 
+    square = lax.broadcasted_iota(jnp.int32, (keep, keep), 0) == lax.broadcasted_iota(
+        jnp.int32, (keep, keep), 1
+    )
+
+    def column(ref, k):
+        row = jnp.broadcast_to(ref[k : k + 1, :].astype(F32), (keep, keep))
+        return jnp.sum(jnp.where(square, row, 0.0), axis=1, keepdims=True)
+
     def route(ref):
-        hots = [(ref[:, k : k + 1] == lane).astype(F32) for k in range(top_k)]
+        ids = [column(ref, k) for k in range(top_k)]
+        hots = [(e == lane).astype(F32) for e in ids]
         before = jnp.dot(lower, sum(hots).astype(BF16), preferred_element_type=F32)
         picks = []
         for k in range(top_k):
             rank = jnp.sum(hots[k] * before, axis=1, keepdims=True)
-            at = ref[:, k : k + 1] - base
+            at = ids[k] - base_f
             here = (at >= 0) & (at < half)
-            rel = at - mine
+            rel = at - mine_f
             rel = jnp.where(rel < 0, rel + half, rel)
-            slot = jnp.where(here, rel.astype(F32) * float(cap) + rank, -1.0)
+            slot = jnp.where(here, rel * float(cap) + rank, -1.0)
             picks.append((slot == slot_lane).astype(BF16))
         return picks
 
     picks = route(ids_ref)
 
-    for c in halo:
-        c.wait()
+    for i in range(0, len(halo), 2):
+        if_left(halo[i].wait_recv)
+        if_right(halo[i + 1].wait_recv)
 
     eye = lax.broadcasted_iota(jnp.int32, (RADIUS, RADIUS), 0) == lax.broadcasted_iota(
         jnp.int32, (RADIUS, RADIUS), 1
@@ -244,6 +277,10 @@
     attsend[...] = attend(other)
     att_copy = remote(attsend, att.at[tp], att_send_sem, att_recv_sem, partner)
     att_copy.start()
+    for c in weights:
+        c.start()
+    for c in local_copies[2:]:
+        c.start()
     att[tp] = attend(tp)
 
     for c in local_copies[:2]:
@@ -349,10 +386,6 @@
 
     experts(slice(0, n_slots), n_slots)
 
-    @pl.loop(1, half)
-    def _(o):
-        home(o).start()
-
     back[0:cap, :] = ret[0:cap, :]
 
     group = max(1, min(half, 128 // cap))
@@ -377,12 +410,16 @@
                 def _():
                     home2(g * group + i, c).start()
 
+    @pl.loop(1, half)
+    def _(o):
+        home(o).start()
+
     back[n_slots : n_slots + cap, :] = ret[n_slots : n_slots + cap, :]
 
     def gathered(chosen, weight_ref, first, cs):
         chunk = back[first : first + n_slots, cs]
         return sum(
-            weight_ref[:, k : k + 1] * jnp.dot(chosen[k], chunk, preferred_element_type=F32)
+            column(weight_ref, k) * jnp.dot(chosen[k], chunk, preferred_element_type=F32)
             for k in range(top_k)
         )
 
@@ -410,6 +447,9 @@
         cs = slice(c * wide, (c + 1) * wide)
         out_ref[:, cs] = (mixed[:, cs] + got[:, cs].astype(F32)).astype(BF16)
 
+    for i in range(0, len(halo), 2):
+        if_right(halo[i].wait_send)
+        if_left(halo[i + 1].wait_send)
     for c in range(parts):
         swaps[c].wait_send()
         crossings[c].wait_send()
@@ -479,8 +519,8 @@
             dma((parts,)),
             dma((2,)),
             dma((2,)),
-            pltpu.VMEM(ids.shape, jnp.int32),
-            pltpu.VMEM(rw.shape, F32),
+            pltpu.VMEM(ids.shape[::-1], jnp.int32),
+            pltpu.VMEM(rw.shape[::-1], F32),
             pltpu.VMEM((keep, dim), BF16),
             pltpu.VMEM((keep, dim), BF16),
             pltpu.VMEM((keep, dim), BF16),
@@ -501,8 +541,8 @@
         w_gate,
         w_up,
         w_down,
-        ids,
-        rw,
+        ids.T,
+        rw.T,
     )
 
 

time: 112 us -> 93.5 us (0.83)
  Pallas kernels: 107 us -> 91.4 us
  local copies, waits for them, and re-layouts: 4.7 us -> 1.88 us
    pallas_call x1, Pallas kernels: 107 us -> 91.4 us  [local(): pl.pallas_call(functools.partial(kernel, n_sp, n_tp, cap, parts), out_sha...]
    unnamed x3 -> x1, local copies, waits for them, and re-layouts: 4.7 us -> 1.88 us
where the time goes in v3:
time: 93.5 us; the launch traced here: 93.3 us
  Pallas kernels  91.4 us (98%)
  local copies, waits for them, and re-layouts  1.88 us (2%)
    pallas_call x1, Pallas kernels, local(): pl.pallas_call(functools.partial(kernel, n_sp, n_tp, cap, parts), out_sha...  91.4 us
    unnamed x1, local copies, waits for them, and re-layouts  1.88 us

profile of v3, /device:TPU:0, one launch (start us, length us, event | category | flops | bytes accessed | tf_op | source)
XLA Modules:
  0.0 93.3 jit_solution(14015080535241764199)
XLA Ops:
  0.0 91.4 %shard_map.127 = bf16[128,2048]{1,0:T(8,128)(2,1)} custom-call(bf16[128,2048]{1,0:T(8,128)(2,1)} %resid_hbm.1, bf16[256,512]{1,0:T(8,128)(2,1)} %q_ref.1, bf16[256,128]{1,0:T(8,128)(2,1)} %k_ref.1, bf16[256,128]{1,0:T(8,128)(2,1)} %v_ref.1, s32[2,1,128]{2,1,0:T(1,128)} %bitcast.6, f32[1,4]{1,0:T(1,128)} %bitcast.9, bf16[1024,2048]{1,0:T(8,128)(2,1)} %wout_hbm.1, ...), custom_call_target="tpu_custom_call" | custom-call | tf_op jit(solution)/shard_map/pallas_call | solution.py:480
  91.5 1.9 %copy.15 = bf16[128,2048]{1,0:T(8,128)(2,1)} copy(bf16[128,2048]{1,0:T(8,128)(2,1)} %shard_map.127) | data formatting | bytes 1048576
